TPU v7x, 32 devices: a whole 2x2x4 slice. The times are simulated.
32 devices in a mesh: sp: 8 (over z, y), tp: 4 (over x, core).
Axes of the slice: x: 2, y: 2, z: 4, core: 2. Of those that a mesh axis runs over, the one named last changes fastest.
Arguments:
- tokens: bfloat16 [3072, 2048], P('sp', 'tp'), may hold values from -6 to 6
- norm_gain: float32 [3, 2048], replicated, may hold values from 0.1 to 1.9
- w_value: bfloat16 [3, 2048, 1024], P(None, 'sp', 'tp'), may hold values from -0.125 to 0.125
- w_gate: bfloat16 [3, 2048, 1024], P(None, 'sp', 'tp'), may hold values from -0.125 to 0.125
- conv_taps: float32 [3, 31, 1024], P(None, None, 'tp'), may hold values from -2.4 to 2.4
- conv_bias: float32 [3, 1024], P(None, 'tp'), may hold values from -3 to 3
- ln_gain: float32 [3, 1024], P(None, 'tp'), may hold values from 0.1 to 1.9
- ln_shift: float32 [3, 1024], P(None, 'tp'), may hold values from -3 to 3
- w_out: bfloat16 [3, 1024, 2048], P(None, 'tp', 'sp'), may hold values from -0.1875 to 0.1875
Outputs:
- stream: bfloat16 [3072, 2048], P('sp', 'tp')
All inputs are finite; a program needn't handle non-finite values.
Results may differ from a plain program's by a relative error of at most 0.015.
Values may be sent and summed in bfloat16 or wider, within the bound.
A program may use at most 64 MiB of HBM per device.

v0:
```python
import jax
import jax.numpy as jnp
from jax import lax
from jax.sharding import PartitionSpec as P

norm_floor = 0.01


def with_halo(array, sides, width):
    for axis, dim in sides:
        size, length = (lax.axis_size(axis), array.shape[dim])
        up = [(i, (i + 1) % size) for i in range(size - 1)]
        down = [(j, i) for i, j in up]
        last = lax.slice_in_dim(array, length - width, length, axis=dim)
        first = lax.slice_in_dim(array, 0, width, axis=dim)
        before = lax.ppermute(last, axis, up)
        after = lax.ppermute(first, axis, down)
        array = jnp.concatenate([before, array, after], axis=dim)
    return array


def body(tokens, norm_gain, w_value, w_gate, conv_taps, conv_bias, ln_gain, ln_shift, w_out):
    stream = tokens
    layer_count = w_value.shape[0]
    reach = conv_taps.shape[1] // 2
    local_channels = w_value.shape[2]
    channels = local_channels * lax.axis_size("tp")
    tok_rows = tokens.shape[0]
    whole_value, whole_gate = (
        lax.all_gather(w_value, "sp", axis=1, tiled=True),
        lax.all_gather(w_gate, "sp", axis=1, tiled=True),
    )
    whole_out = lax.all_gather(w_out, "sp", axis=2, tiled=True)
    for layer_index in range(layer_count):
        whole_rows = lax.all_gather(stream, "tp", axis=1, tiled=True)
        rows_f32 = whole_rows.astype(jnp.float32)
        scale_rows = lax.rsqrt(jnp.mean(rows_f32 * rows_f32, axis=-1, keepdims=True) + norm_floor)
        normed = (rows_f32 * scale_rows * norm_gain[layer_index]).astype(jnp.bfloat16)
        value_rows = jnp.dot(normed, whole_value[layer_index], preferred_element_type=jnp.float32)
        gate_rows = jnp.dot(normed, whole_gate[layer_index], preferred_element_type=jnp.float32)
        gated_input = (value_rows * jax.nn.sigmoid(gate_rows)).astype(jnp.bfloat16)
        padded = with_halo(gated_input, (("sp", 0),), reach)
        padded = padded.astype(jnp.float32)
        convolved = jnp.zeros((tok_rows, local_channels), jnp.float32) + conv_bias[layer_index]
        for offset in range(2 * reach + 1):
            convolved = (
                convolved + conv_taps[layer_index, offset] * padded[offset : offset + tok_rows]
            )
        moments = lax.psum(
            (
                jnp.sum(convolved, axis=-1, keepdims=True),
                jnp.sum(convolved * convolved, axis=-1, keepdims=True),
            ),
            "tp",
        )
        average = moments[0] / channels
        spread = moments[1] / channels - average * average
        activated = jax.nn.silu(
            (convolved - average) * lax.rsqrt(spread + norm_floor) * ln_gain[layer_index]
            + ln_shift[layer_index]
        ).astype(jnp.bfloat16)
        partial_rows = jnp.dot(
            activated, whole_out[layer_index], preferred_element_type=jnp.float32
        )
        summed = lax.psum_scatter(
            partial_rows.astype(jnp.bfloat16), "tp", scatter_dimension=1, tiled=True
        ).astype(jnp.float32)
        stream = (stream.astype(jnp.float32) + summed).astype(jnp.bfloat16)
    return stream


def solution(mesh):
    placed = (
        P("sp", "tp"),
        P(),
        P(None, "sp", "tp"),
        P(None, "sp", "tp"),
        P(None, None, "tp"),
        P(None, "tp"),
        P(None, "tp"),
        P(None, "tp"),
        P(None, "tp", "sp"),
    )
    return jax.shard_map(body, mesh=mesh, in_specs=placed, out_specs=P("sp", "tp"), check_vma=False)
```

profile of v0, /device:TPU:0, one launch (start us, length us, event | category | flops | bytes accessed | tf_op | source)
XLA Modules:
  0.0 407.2 jit_solution(14767884248414049821)
XLA Ops:
  6.5 0.7 all-gather.7.cloned.1.call-update
  7.3 0.0 all-gather.11.cloned.1.call-start
  7.3 0.7 all-gather.11.cloned.1.call-update
  8.0 0.0 all-gather.9.cloned.1.call-start
  8.1 0.7 all-gather.9.cloned.1.call-update
  8.7 0.0 all-gather.13.cloned.1.call-start
  8.8 0.5 all-gather.13.cloned.1.call-update
  9.3 0.0 reduce-scatter.4.cloned.1.call-start
  9.4 0.8 fusion.155
  10.2 0.8 fusion.153
  11.0 1.0 fusion.151
  12.0 1.1 fusion.150
  13.0 0.9 fusion.152
  13.9 17.3 %all-gather.7.cloned.1.call-done = bf16[384,2048]{1,0:T(8,128)(2,1)} async-done(((bf16[384,512]{1,0:T(8,128)(2,1)}), bf16[384,2048]{1,0:T(8,128)(2,1)}) %all-gather.7.cloned.1.call-update) | async-done | bytes 1572880 | tf_op jit(solution)/shard_map/all_gather | solution.py:35
  31.3 1.8 fusion
  33.1 60.4 %all-gather.11.cloned.1.call-done = bf16[3,2048,256]{2,1,0:T(8,128)(2,1)} async-done(((bf16[3,256,256]{2,1,0:T(8,128)(2,1)}), bf16[3,2048,256]{2,1,0:T(8,128)(2,1)}) %all-gather.11.cloned.1.call-update) | async-done | bytes 3145744 | tf_op jit(solution)/shard_map/all_gather | solution.py:31
  93.5 2.5 fusion.13
  96.0 0.0 copy-start.7
  96.0 58.4 %all-gather.9.cloned.1.call-done = bf16[3,2048,256]{2,1,0:T(8,128)(2,1)} async-done(((bf16[3,256,256]{2,1,0:T(8,128)(2,1)}), bf16[3,2048,256]{2,1,0:T(8,128)(2,1)}) %all-gather.9.cloned.1.call-update) | async-done | bytes 3145744 | tf_op jit(solution)/shard_map/all_gather | solution.py:30
  154.4 1.9 fusion.18
  156.3 2.5 collective-permute-start
  158.8 1.3 collective-permute-start.1
  160.1 0.0 collective-permute-done
  160.1 4.6 %collective-permute-done.1 = bf16[15,256]{1,0:T(8,128)(2,1)S(1)} collective-permute-done((bf16[15,256]{1,0:T(8,128)(2,1)S(1)}, bf16[15,256]{1,0:T(8,128)(2,1)S(1)}, u32[]{:S(2)}, u32[]{:S(2)}) %collective-permute-start.1) | collective-permute-done | bytes 7712 | tf_op jit(solution)/shard_map/ppermute | solution.py:17
  164.7 1.7 fusion.140
  166.4 6.2 %all-reduce.2 = (f32[384,1]{0,1:T(1,128)S(1)}, f32[384,1]{0,1:T(1,128)S(1)}) all-reduce(f32[384,1]{0,1:T(1,128)S(1)} %broadcast_in_dim.21, f32[384,1]{0,1:T(1,128)S(1)} %broadcast_in_dim.22), channel_id=1, replica_groups=mesh['sp'=8,'tp'=4] {'tp'}, use_global_device_ids=true, to_apply=%region_2.0 | all-reduce | flops 768 | bytes 6144 | tf_op jit(solution)/shard_map/psum | solution.py:49
  172.7 45.0 %all-gather.13.cloned.1.call-done = bf16[3,256,2048]{2,1,0:T(8,128)(2,1)} async-done(((bf16[3,256,256]{2,1,0:T(8,128)(2,1)}), bf16[3,256,2048]{2,1,0:T(8,128)(2,1)}) %all-gather.13.cloned.1.call-update) | async-done | bytes 3145744 | tf_op jit(solution)/shard_map/all_gather | solution.py:33
  217.7 3.1 convolution_convert_fusion.2
  220.8 0.0 reduce-scatter.4.cloned.1.call-update
  220.8 0.0 all-gather.15.cloned.1.call-start
  220.8 26.3 %reduce-scatter.4.cloned.1.call-done = bf16[384,512]{1,0:T(8,128)(2,1)} async-done(((bf16[384,2048]{1,0:T(8,128)(2,1)}), bf16[384,512]{1,0:T(8,128)(2,1)}) %reduce-scatter.4.cloned.1.call-update) | async-done | bytes 393232 | tf_op jit(solution)/shard_map/reduce_scatter | solution.py:65
  247.2 1.8 add_convert_fusion.2
  249.0 0.0 all-gather.15.cloned.1.call-update
  249.0 0.0 reduce-scatter.6.cloned.1.call-start
  249.1 19.7 %all-gather.15.cloned.1.call-done = bf16[384,2048]{1,0:T(8,128)(2,1)} async-done(((bf16[384,512]{1,0:T(8,128)(2,1)}), bf16[384,2048]{1,0:T(8,128)(2,1)}) %all-gather.15.cloned.1.call-update) | async-done | bytes 1572880 | tf_op jit(solution)/shard_map/all_gather | solution.py:35
  268.8 1.8 fusion.3
  270.6 2.5 fusion.15
  273.1 1.9 fusion.19
  275.0 3.4 collective-permute-start.2
  278.4 1.3 collective-permute-start.3
  279.7 0.0 collective-permute-done.2
  279.7 4.2 %collective-permute-done.3 = bf16[15,256]{1,0:T(8,128)(2,1)S(1)} collective-permute-done((bf16[15,256]{1,0:T(8,128)(2,1)S(1)}, bf16[15,256]{1,0:T(8,128)(2,1)S(1)}, u32[]{:S(2)}, u32[]{:S(2)}) %collective-permute-start.3) | collective-permute-done | bytes 7712 | tf_op jit(solution)/shard_map/ppermute | solution.py:17
  284.0 1.7 fusion.139
  285.7 6.1 %all-reduce.1 = (f32[384,1]{0,1:T(1,128)S(1)}, f32[384,1]{0,1:T(1,128)S(1)}) all-reduce(f32[384,1]{0,1:T(1,128)S(1)} %broadcast_in_dim.23, f32[384,1]{0,1:T(1,128)S(1)} %broadcast_in_dim.24), channel_id=1, replica_groups=mesh['sp'=8,'tp'=4] {'tp'}, use_global_device_ids=true, to_apply=%region_8.9 | all-reduce | flops 768 | bytes 6144 | tf_op jit(solution)/shard_map/psum | solution.py:49
  291.8 3.1 convolution_convert_fusion.1
  294.8 0.0 reduce-scatter.6.cloned.1.call-update
  294.9 0.0 all-gather.17.cloned.1.call-start
  294.9 28.1 %reduce-scatter.6.cloned.1.call-done = bf16[384,512]{1,0:T(8,128)(2,1)} async-done(((bf16[384,2048]{1,0:T(8,128)(2,1)}), bf16[384,512]{1,0:T(8,128)(2,1)}) %reduce-scatter.6.cloned.1.call-update) | async-done | bytes 393232 | tf_op jit(solution)/shard_map/reduce_scatter | solution.py:65
  323.0 1.8 add_convert_fusion.1
  324.8 0.0 all-gather.17.cloned.1.call-update
  324.9 0.0 reduce-scatter.8.cloned.1.call-start
  324.9 19.7 %all-gather.17.cloned.1.call-done = bf16[384,2048]{1,0:T(8,128)(2,1)} async-done(((bf16[384,512]{1,0:T(8,128)(2,1)}), bf16[384,2048]{1,0:T(8,128)(2,1)}) %all-gather.17.cloned.1.call-update) | async-done | bytes 1572880 | tf_op jit(solution)/shard_map/all_gather | solution.py:35
  344.6 1.8 fusion.6
  346.4 2.5 fusion.17
  348.9 1.9 fusion.20
  350.8 3.4 collective-permute-start.4
  354.2 1.5 collective-permute-start.5
  355.7 4.0 collective-permute-done.5
  359.8 1.7 fusion.138
  361.5 6.1 %all-reduce = (f32[384,1]{0,1:T(1,128)S(1)}, f32[384,1]{0,1:T(1,128)S(1)}) all-reduce(f32[384,1]{0,1:T(1,128)S(1)} %broadcast_in_dim.25, f32[384,1]{0,1:T(1,128)S(1)} %broadcast_in_dim.26), channel_id=1, replica_groups=mesh['sp'=8,'tp'=4] {'tp'}, use_global_device_ids=true, to_apply=%region_14.15 | all-reduce | flops 768 | bytes 6144 | tf_op jit(solution)/shard_map/psum | solution.py:49
  367.6 3.0 convolution_convert_fusion
  370.6 0.0 reduce-scatter.8.cloned.1.call-update
  370.7 28.2 %reduce-scatter.8.cloned.1.call-done = bf16[384,512]{1,0:T(8,128)(2,1)} async-done(((bf16[384,2048]{1,0:T(8,128)(2,1)}), bf16[384,512]{1,0:T(8,128)(2,1)}) %reduce-scatter.8.cloned.1.call-update) | async-done | bytes 393232 | tf_op jit(solution)/shard_map/reduce_scatter | solution.py:65
  398.9 1.8 add_convert_fusion
  (39 shorter events, 0.4 us)
Async XLA Ops:
  6.5 24.7 %all-gather.7.cloned.1.call-start = ((), (), s32[]{:S(2)}) async-start(), calls=%async_computation.3 | async-start | bytes 1966080 | tf_op jit(solution)/shard_map/all_gather | solution.py:35
  7.3 86.3 %all-gather.11.cloned.1.call-start = ((), (), s32[]{:S(2)}) async-start(), calls=%async_computation.5 | async-start | bytes 3538944 | tf_op jit(solution)/shard_map/all_gather | solution.py:31
  8.0 146.4 %all-gather.9.cloned.1.call-start = ((), (), s32[]{:S(2)}) async-start(), calls=%async_computation.4 | async-start | bytes 3538944 | tf_op jit(solution)/shard_map/all_gather | solution.py:30
  8.7 208.9 %all-gather.13.cloned.1.call-start = ((), (), s32[]{:S(2)}) async-start(), calls=%async_computation.6 | async-start | bytes 3538944 | tf_op jit(solution)/shard_map/all_gather | solution.py:33
  9.3 237.9 %reduce-scatter.4.cloned.1.call-start = ((), (), s32[]{:S(2)}) async-start(), calls=%async_computation.7 | async-start | bytes 1966080 | tf_op jit(solution)/shard_map/reduce_scatter | solution.py:65
  93.5 60.9 %copy-start.2 = (bf16[384,2048]{1,0:T(8,128)(2,1)S(1)}, bf16[384,2048]{1,0:T(8,128)(2,1)}, u32[]{:S(2)}) copy-start(bf16[384,2048]{1,0:T(8,128)(2,1)} %all-gather.7.cloned.1.call-done) | copy-start | bytes 4718596
  96.0 64.1 %copy-start.7 = (f32[3,256]{1,0:T(4,128)S(1)}, f32[3,256]{1,0:T(4,128)}, u32[]{:S(2)}) copy-start(f32[3,256]{1,0:T(4,128)} %param.16) | copy-start | bytes 9220
  156.3 3.8 collective-permute-start
  158.8 5.9 %collective-permute-start.1 = (bf16[15,256]{1,0:T(8,128)(2,1)S(1)}, bf16[15,256]{1,0:T(8,128)(2,1)S(1)}, u32[]{:S(2)}, u32[]{:S(2)}) collective-permute-start(bf16[15,256]{1,0:T(8,128)(2,1)S(1)} %get-tuple-element.31), channel_id=1, source_target_pairs={{4,0},{8,4},{12,8},{16,12},{20,16},{24,20},{28,24},{5,1},{9,5},{13... | collective-permute-start | bytes 23048 | tf_op jit(solution)/shard_map/ppermute | solution.py:17
  166.4 80.7 %copy-start.5 = (bf16[384,512]{1,0:T(8,128)(2,1)S(1)}, bf16[384,512]{1,0:T(8,128)(2,1)}, u32[]{:S(2)}) copy-start(bf16[384,512]{1,0:T(8,128)(2,1)} %param.9) | copy-start | bytes 1179652
  217.7 31.4 %copy-start.6 = (f32[3,31,256]{2,1,0:T(8,128)S(1)}, f32[3,31,256]{2,1,0:T(8,128)}, u32[]{:S(2)}) copy-start(f32[3,31,256]{2,1,0:T(8,128)} %param.13) | copy-start | bytes 285700
  220.8 48.0 %all-gather.15.cloned.1.call-start = ((), (), s32[]{:S(2)}) async-start(), calls=%async_computation.8 | async-start | bytes 1966080 | tf_op jit(solution)/shard_map/all_gather | solution.py:35
  249.0 74.0 %reduce-scatter.6.cloned.1.call-start = ((), (), s32[]{:S(2)}) async-start(), calls=%async_computation.9 | async-start | bytes 1966080 | tf_op jit(solution)/shard_map/reduce_scatter | solution.py:65
  270.6 2.5 copy-start.3
  275.0 4.7 %collective-permute-start.2 = (bf16[15,256]{1,0:T(8,128)(2,1)S(1)}, bf16[15,256]{1,0:T(8,128)(2,1)S(1)}, u32[]{:S(2)}, u32[]{:S(2)}) collective-permute-start(bf16[15,256]{1,0:T(8,128)(2,1)S(1)} %get-tuple-element.28), channel_id=1, source_target_pairs={{0,4},{4,8},{8,12},{12,16},{16,20},{20,24},{24,28},{1,5},{5,9},{9,... | collective-permute-start | bytes 23048 | tf_op jit(solution)/shard_map/ppermute | solution.py:16
  278.4 5.5 %collective-permute-start.3 = (bf16[15,256]{1,0:T(8,128)(2,1)S(1)}, bf16[15,256]{1,0:T(8,128)(2,1)S(1)}, u32[]{:S(2)}, u32[]{:S(2)}) collective-permute-start(bf16[15,256]{1,0:T(8,128)(2,1)S(1)} %get-tuple-element.29), channel_id=1, source_target_pairs={{4,0},{8,4},{12,8},{16,12},{20,16},{24,20},{28,24},{5,1},{9,5},{13... | collective-permute-start | bytes 23048 | tf_op jit(solution)/shard_map/ppermute | solution.py:17
  285.7 37.3 %copy-start = (bf16[384,512]{1,0:T(8,128)(2,1)S(1)}, bf16[384,512]{1,0:T(8,128)(2,1)}, u32[]{:S(2)}) copy-start(bf16[384,512]{1,0:T(8,128)(2,1)} %add_convert_fusion.2) | copy-start | bytes 1179652
  294.9 49.8 %all-gather.17.cloned.1.call-start = ((), (), s32[]{:S(2)}) async-start(), calls=%async_computation.10 | async-start | bytes 1966080 | tf_op jit(solution)/shard_map/all_gather | solution.py:35
  324.9 74.0 %reduce-scatter.8.cloned.1.call-start = ((), (), s32[]{:S(2)}) async-start(), calls=%async_computation.11 | async-start | bytes 1966080 | tf_op jit(solution)/shard_map/reduce_scatter | solution.py:65
  346.4 2.5 copy-start.4
  350.8 4.9 %collective-permute-start.4 = (bf16[15,256]{1,0:T(8,128)(2,1)S(1)}, bf16[15,256]{1,0:T(8,128)(2,1)S(1)}, u32[]{:S(2)}, u32[]{:S(2)}) collective-permute-start(bf16[15,256]{1,0:T(8,128)(2,1)S(1)} %get-tuple-element.26), channel_id=1, source_target_pairs={{0,4},{4,8},{8,12},{12,16},{16,20},{20,24},{24,28},{1,5},{5,9},{9,... | collective-permute-start | bytes 23048 | tf_op jit(solution)/shard_map/ppermute | solution.py:16
  354.2 5.5 %collective-permute-start.5 = (bf16[15,256]{1,0:T(8,128)(2,1)S(1)}, bf16[15,256]{1,0:T(8,128)(2,1)S(1)}, u32[]{:S(2)}, u32[]{:S(2)}) collective-permute-start(bf16[15,256]{1,0:T(8,128)(2,1)S(1)} %get-tuple-element.27), channel_id=1, source_target_pairs={{4,0},{8,4},{12,8},{16,12},{20,16},{24,20},{28,24},{5,1},{9,5},{13... | collective-permute-start | bytes 23048 | tf_op jit(solution)/shard_map/ppermute | solution.py:17
  361.5 37.4 %copy-start.1 = (bf16[384,512]{1,0:T(8,128)(2,1)S(1)}, bf16[384,512]{1,0:T(8,128)(2,1)}, u32[]{:S(2)}) copy-start(bf16[384,512]{1,0:T(8,128)(2,1)} %add_convert_fusion.1) | copy-start | bytes 1179652
Sparse Core Ops, SparseCore 0:
  8.9 22.3 all-gather.6
  33.5 60.0 all-gather.10
  95.7 58.6 all-gather.8
  156.3 61.2 all-gather.12
  220.9 26.2 reduce-scatter.3
  249.2 19.6 all-gather.14
  295.0 27.9 reduce-scatter.5
  325.0 19.6 all-gather.16
  370.8 28.0 reduce-scatter.7
where the time goes:
time: 408 us; the launch traced here: 407 us
  waiting for transfers between devices  319 us (78%)
  matrix products  22.1 us (5%)
  blocking collectives  18.4 us (5%)
  other arithmetic  16.2 us (4%)
  starting transfers between devices  13.6 us (3%)
  between operations  13.5 us (3%)
  local copies, waits for them, and re-layouts  4.71 us (1%)
    reduce_scatter x3, waiting for transfers between devices, body(): lax.psum_scatter(partial_rows.astype(jnp.bfloat16), 'tp', scatter_dimensi...  82.6 us
    all_gather x1, waiting for transfers between devices, body(): lax.all_gather(w_gate, 'sp', axis=1, tiled=True)  60.4 us
    all_gather x1, waiting for transfers between devices, body(): lax.all_gather(w_value, 'sp', axis=1, tiled=True)  58.4 us
    all_gather x3, waiting for transfers between devices, body(): whole_rows = lax.all_gather(stream, 'tp', axis=1, tiled=True)  56.8 us
    all_gather x1, waiting for transfers between devices, body(): whole_out = lax.all_gather(w_out, 'sp', axis=2, tiled=True)  45 us
    psum x3, blocking collectives, body(): lax.psum((jnp.sum(convolved, axis=-1, keepdims=True), jnp.sum(convolved *...  18.4 us
    ppermute x3, waiting for transfers between devices, with_halo(): after = lax.ppermute(first, axis, down)  12.8 us
    ppermute x3, starting transfers between devices, with_halo(): before = lax.ppermute(last, axis, up)  9.21 us
  transfers between devices with their start and end apart: 15, of which 12 were waited for; matrix products, arithmetic and copies ran while one was open for 3% of the time, Pallas kernels for 0%

commit v1 on v0

--- a/solution.py
+++ b/solution.py
@@ -32,7 +32,14 @@
     )
     whole_out = lax.all_gather(w_out, "sp", axis=2, tiled=True)
     for layer_index in range(layer_count):
-        whole_rows = lax.all_gather(stream, "tp", axis=1, tiled=True)
+        ring = [stream]
+        for hop in range(3):
+            ring.append(lax.ppermute(ring[-1], "tp", [(dev, (dev + 1) % 4) for dev in range(4)]))
+        whole_rows = jnp.roll(
+            jnp.concatenate(ring[::-1], axis=1),
+            (lax.axis_index("tp") + 1) * ring[0].shape[1],
+            axis=1,
+        )
         rows_f32 = whole_rows.astype(jnp.float32)
         scale_rows = lax.rsqrt(jnp.mean(rows_f32 * rows_f32, axis=-1, keepdims=True) + norm_floor)
         normed = (rows_f32 * scale_rows * norm_gain[layer_index]).astype(jnp.bfloat16)

time: 408 us -> 393 us (0.963)
  waiting for transfers between devices: 319 us -> 298 us
  other arithmetic: 16.2 us -> 22.9 us
    ppermute x0 -> x9, waiting for transfers between devices: none -> 60.5 us  [body(): lax.ppermute(ring[-1], 'tp', [(dev, (dev + 1) % 4) for dev in range(4)])]
    all_gather x3 -> x0, waiting for transfers between devices: 56.8 us -> none  [body(): whole_rows = lax.all_gather(stream, 'tp', axis=1, tiled=True)]
    all_gather x1, waiting for transfers between devices: 60.4 us -> 36.1 us  [body(): lax.all_gather(w_gate, 'sp', axis=1, tiled=True)]
    reduce_sum x3, other arithmetic: 5.37 us -> 13.6 us  [body(): jnp.mean(rows_f32 * rows_f32, axis=-1, keepdims=True) + norm_floor]
  transfers between devices with their start and end apart: 15 -> 21, of which waited for: 12 -> 18; matrix products, arithmetic and copies ran while one was open for 3% -> 4% of each run, Pallas kernels for 0% -> 0%
where the time goes in v1:
time: 393 us; the launch traced here: 392 us
  waiting for transfers between devices  298 us (76%)
  other arithmetic  22.9 us (6%)
  matrix products  20.5 us (5%)
  blocking collectives  18.1 us (5%)
  starting transfers between devices  14.2 us (4%)
  between operations  13.8 us (4%)
  local copies, waits for them, and re-layouts  4.71 us (1%)
    reduce_scatter x3, waiting for transfers between devices, body(): lax.psum_scatter(partial_rows.astype(jnp.bfloat16), 'tp', scatter_dimensi...  82.6 us
    ppermute x9, waiting for transfers between devices, body(): lax.ppermute(ring[-1], 'tp', [(dev, (dev + 1) % 4) for dev in range(4)])  60.5 us
    all_gather x1, waiting for transfers between devices, body(): lax.all_gather(w_value, 'sp', axis=1, tiled=True)  59 us
    all_gather x1, waiting for transfers between devices, body(): whole_out = lax.all_gather(w_out, 'sp', axis=2, tiled=True)  45.2 us
    all_gather x1, waiting for transfers between devices, body(): lax.all_gather(w_gate, 'sp', axis=1, tiled=True)  36.1 us
    psum x3, blocking collectives, body(): lax.psum((jnp.sum(convolved, axis=-1, keepdims=True), jnp.sum(convolved *...  18.1 us
    reduce_sum x3, other arithmetic, body(): jnp.mean(rows_f32 * rows_f32, axis=-1, keepdims=True) + norm_floor  13.6 us
    ppermute x3, waiting for transfers between devices, with_halo(): after = lax.ppermute(first, axis, down)  12.8 us
  transfers between devices with their start and end apart: 21, of which 18 were waited for; matrix products, arithmetic and copies ran while one was open for 4% of the time, Pallas kernels for 0%

profile of v1, /device:TPU:0, one launch (start us, length us, event | category | flops | bytes accessed | tf_op | source)
XLA Modules:
  0.0 392.4 jit_solution(7051915566808441754)
XLA Ops:
  6.5 0.7 all-gather.6.cloned.1.call-update
  7.3 0.0 all-gather.4.cloned.1.call-start
  7.3 0.7 all-gather.4.cloned.1.call-update
  8.0 0.0 all-gather.8.cloned.1.call-start
  8.1 0.7 all-gather.8.cloned.1.call-update
  8.7 0.0 reduce-scatter.4.cloned.1.call-start
  8.8 0.5 collective-permute-start
  9.3 0.8 fusion.179
  10.1 1.0 fusion.175
  11.1 5.8 %collective-permute-done = bf16[384,512]{1,0:T(8,128)(2,1)S(1)} collective-permute-done((bf16[384,512]{1,0:T(8,128)(2,1)}, bf16[384,512]{1,0:T(8,128)(2,1)S(1)}, u32[]{:S(2)}, u32[]{:S(2)}) %collective-permute-start) | collective-permute-done | bytes 393248 | tf_op jit(solution)/shard_map/ppermute | solution.py:37
  16.9 0.0 collective-permute-start.1
  17.0 0.8 fusion.177
  17.8 1.1 fusion.174
  18.9 5.3 %collective-permute-done.1 = bf16[384,512]{1,0:T(8,128)(2,1)S(1)} collective-permute-done((bf16[384,512]{1,0:T(8,128)(2,1)S(1)}, bf16[384,512]{1,0:T(8,128)(2,1)S(1)}, u32[]{:S(2)}, u32[]{:S(2)}) %collective-permute-start.1) | collective-permute-done | bytes 393248 | tf_op jit(solution)/shard_map/ppermute | solution.py:37
  24.1 0.9 fusion.176
  25.0 6.3 %collective-permute-done.2 = bf16[384,512]{1,0:T(8,128)(2,1)S(1)} collective-permute-done((bf16[384,512]{1,0:T(8,128)(2,1)S(1)}, bf16[384,512]{1,0:T(8,128)(2,1)S(1)}, u32[]{:S(2)}, u32[]{:S(2)}) %collective-permute-start.2) | collective-permute-done | bytes 393248 | tf_op jit(solution)/shard_map/ppermute | solution.py:37
  31.3 4.9 %fusion = (f32[384]{0:T(512)S(1)}, bf16[384,2048]{1,0:T(8,128)(2,1)S(1)}) fusion(s32[]{:T(128)S(6)} %select_n.15, bf16[384,512]{1,0:T(8,128)(2,1)} %param.11, bf16[384,512]{1,0:T(8,128)(2,1)S(1)} %collective-permute-done, bf16[384,512]{1,0:T(8,128)(2,1)S(1)} %collective-permute-done.1, bf16[384,512]{1,0:T(8,128)(2,1)S(1)} %collective-permute-done.2), kind=kLoop, calls=%fused_computation.6 | loop fusion | flops 14941824 | bytes 3147268 | tf_op jit(solution)/shard_map/reduce_sum | solution.py:44
  36.2 36.1 %all-gather.6.cloned.1.call-done = bf16[3,2048,256]{2,1,0:T(8,128)(2,1)} async-done(((bf16[3,256,256]{2,1,0:T(8,128)(2,1)}), bf16[3,2048,256]{2,1,0:T(8,128)(2,1)}) %all-gather.6.cloned.1.call-update) | async-done | bytes 3145744 | tf_op jit(solution)/shard_map/all_gather | solution.py:31
  72.3 1.9 fusion.34
  74.2 59.0 %all-gather.4.cloned.1.call-done = bf16[3,2048,256]{2,1,0:T(8,128)(2,1)} async-done(((bf16[3,256,256]{2,1,0:T(8,128)(2,1)}), bf16[3,2048,256]{2,1,0:T(8,128)(2,1)}) %all-gather.4.cloned.1.call-update) | async-done | bytes 3145744 | tf_op jit(solution)/shard_map/all_gather | solution.py:30
  133.2 1.9 fusion.39
  135.1 2.5 collective-permute-start.3
  137.6 1.3 collective-permute-start.4
  138.9 0.0 collective-permute-done.3
  138.9 4.6 %collective-permute-done.4 = bf16[15,256]{1,0:T(8,128)(2,1)S(1)} collective-permute-done((bf16[15,256]{1,0:T(8,128)(2,1)S(1)}, bf16[15,256]{1,0:T(8,128)(2,1)S(1)}, u32[]{:S(2)}, u32[]{:S(2)}) %collective-permute-start.4) | collective-permute-done | bytes 7712 | tf_op jit(solution)/shard_map/ppermute | solution.py:17
  143.5 1.7 fusion.161
  145.2 6.2 %all-reduce.2 = (f32[384,1]{0,1:T(1,128)S(1)}, f32[384,1]{0,1:T(1,128)S(1)}) all-reduce(f32[384,1]{0,1:T(1,128)S(1)} %broadcast_in_dim.21, f32[384,1]{0,1:T(1,128)S(1)} %broadcast_in_dim.22), channel_id=1, replica_groups=mesh['sp'=8,'tp'=4] {'tp'}, use_global_device_ids=true, to_apply=%region_2.4 | all-reduce | flops 768 | bytes 6144 | tf_op jit(solution)/shard_map/psum | solution.py:56
  151.4 45.2 %all-gather.8.cloned.1.call-done = bf16[3,256,2048]{2,1,0:T(8,128)(2,1)} async-done(((bf16[3,256,256]{2,1,0:T(8,128)(2,1)}), bf16[3,256,2048]{2,1,0:T(8,128)(2,1)}) %all-gather.8.cloned.1.call-update) | async-done | bytes 3145744 | tf_op jit(solution)/shard_map/all_gather | solution.py:33
  196.6 3.1 convolution_convert_fusion.2
  199.7 0.0 reduce-scatter.6.cloned.1.call-start
  199.8 26.3 %reduce-scatter.4.cloned.1.call-done = bf16[384,512]{1,0:T(8,128)(2,1)} async-done(((bf16[384,2048]{1,0:T(8,128)(2,1)}), bf16[384,512]{1,0:T(8,128)(2,1)}) %reduce-scatter.4.cloned.1.call-update) | async-done | bytes 393232 | tf_op jit(solution)/shard_map/reduce_scatter | solution.py:72
  226.1 1.1 add_convert_fusion.2
  227.2 0.1 collective-permute-start.5
  227.3 7.2 %collective-permute-done.5 = bf16[384,512]{1,0:T(8,128)(2,1)S(1)} collective-permute-done((bf16[384,512]{1,0:T(8,128)(2,1)S(1)}, bf16[384,512]{1,0:T(8,128)(2,1)S(1)}, u32[]{:S(2)}, u32[]{:S(2)}) %collective-permute-start.5) | collective-permute-done | bytes 393248 | tf_op jit(solution)/shard_map/ppermute | solution.py:37
  234.4 7.2 %collective-permute-done.6 = bf16[384,512]{1,0:T(8,128)(2,1)S(1)} collective-permute-done((bf16[384,512]{1,0:T(8,128)(2,1)S(1)}, bf16[384,512]{1,0:T(8,128)(2,1)S(1)}, u32[]{:S(2)}, u32[]{:S(2)}) %collective-permute-start.6) | collective-permute-done | bytes 393248 | tf_op jit(solution)/shard_map/ppermute | solution.py:37
  241.7 7.2 %collective-permute-done.7 = bf16[384,512]{1,0:T(8,128)(2,1)S(1)} collective-permute-done((bf16[384,512]{1,0:T(8,128)(2,1)S(1)}, bf16[384,512]{1,0:T(8,128)(2,1)S(1)}, u32[]{:S(2)}, u32[]{:S(2)}) %collective-permute-start.7) | collective-permute-done | bytes 393248 | tf_op jit(solution)/shard_map/ppermute | solution.py:37
  248.8 4.4 %fusion.3 = (f32[384]{0:T(512)S(1)}, bf16[384,2048]{1,0:T(8,128)(2,1)S(1)}) fusion(s32[]{:T(128)S(6)} %select_n.15, bf16[384,512]{1,0:T(8,128)(2,1)S(1)} %add_convert_fusion.2, bf16[384,512]{1,0:T(8,128)(2,1)S(1)} %collective-permute-done.5, bf16[384,512]{1,0:T(8,128)(2,1)S(1)} %collective-permute-done.6, bf16[384,512]{1,0:T(8,128)(2,1)S(1)} %collective-permute-done.7), kind=kLoop, calls=%fused_computation.9 | loop fusion | flops 14941824 | bytes 3147268 | tf_op jit(solution)/shard_map/reduce_sum | solution.py:44
  253.2 1.9 fusion.36
  255.2 1.9 fusion.40
  257.0 3.4 collective-permute-start.8
  260.4 1.5 collective-permute-start.9
  262.0 4.0 %collective-permute-done.9 = bf16[15,256]{1,0:T(8,128)(2,1)S(1)} collective-permute-done((bf16[15,256]{1,0:T(8,128)(2,1)S(1)}, bf16[15,256]{1,0:T(8,128)(2,1)S(1)}, u32[]{:S(2)}, u32[]{:S(2)}) %collective-permute-start.9) | collective-permute-done | bytes 7712 | tf_op jit(solution)/shard_map/ppermute | solution.py:17
  266.0 1.7 fusion.160
  267.7 5.9 %all-reduce.1 = (f32[384,1]{0,1:T(1,128)S(1)}, f32[384,1]{0,1:T(1,128)S(1)}) all-reduce(f32[384,1]{0,1:T(1,128)S(1)} %broadcast_in_dim.23, f32[384,1]{0,1:T(1,128)S(1)} %broadcast_in_dim.24), channel_id=1, replica_groups=mesh['sp'=8,'tp'=4] {'tp'}, use_global_device_ids=true, to_apply=%region_8.10 | all-reduce | flops 768 | bytes 6144 | tf_op jit(solution)/shard_map/psum | solution.py:56
  273.7 3.1 convolution_convert_fusion.1
  276.8 0.0 reduce-scatter.8.cloned.1.call-start
  276.8 28.1 %reduce-scatter.6.cloned.1.call-done = bf16[384,512]{1,0:T(8,128)(2,1)} async-done(((bf16[384,2048]{1,0:T(8,128)(2,1)}), bf16[384,512]{1,0:T(8,128)(2,1)}) %reduce-scatter.6.cloned.1.call-update) | async-done | bytes 393232 | tf_op jit(solution)/shard_map/reduce_scatter | solution.py:72
  304.9 1.1 add_convert_fusion.1
  306.0 0.1 collective-permute-start.10
  306.1 7.2 %collective-permute-done.10 = bf16[384,512]{1,0:T(8,128)(2,1)S(1)} collective-permute-done((bf16[384,512]{1,0:T(8,128)(2,1)S(1)}, bf16[384,512]{1,0:T(8,128)(2,1)S(1)}, u32[]{:S(2)}, u32[]{:S(2)}) %collective-permute-start.10) | collective-permute-done | bytes 393248 | tf_op jit(solution)/shard_map/ppermute | solution.py:37
  313.3 7.2 %collective-permute-done.11 = bf16[384,512]{1,0:T(8,128)(2,1)S(1)} collective-permute-done((bf16[384,512]{1,0:T(8,128)(2,1)S(1)}, bf16[384,512]{1,0:T(8,128)(2,1)S(1)}, u32[]{:S(2)}, u32[]{:S(2)}) %collective-permute-start.11) | collective-permute-done | bytes 393248 | tf_op jit(solution)/shard_map/ppermute | solution.py:37
  320.5 7.2 %collective-permute-done.12 = bf16[384,512]{1,0:T(8,128)(2,1)S(1)} collective-permute-done((bf16[384,512]{1,0:T(8,128)(2,1)S(1)}, bf16[384,512]{1,0:T(8,128)(2,1)S(1)}, u32[]{:S(2)}, u32[]{:S(2)}) %collective-permute-start.12) | collective-permute-done | bytes 393248 | tf_op jit(solution)/shard_map/ppermute | solution.py:37
  327.7 4.4 %fusion.6 = (f32[384]{0:T(512)S(1)}, bf16[384,2048]{1,0:T(8,128)(2,1)S(1)}) fusion(s32[]{:T(128)S(6)} %select_n.15, bf16[384,512]{1,0:T(8,128)(2,1)S(1)} %add_convert_fusion.1, bf16[384,512]{1,0:T(8,128)(2,1)S(1)} %collective-permute-done.10, bf16[384,512]{1,0:T(8,128)(2,1)S(1)} %collective-permute-done.11, bf16[384,512]{1,0:T(8,128)(2,1)S(1)} %collective-permute-done.12), kind=kLoop, calls=%fused_computation.12 | loop fusion | flops 14941824 | bytes 3147268 | tf_op jit(solution)/shard_map/reduce_sum | solution.py:44
  332.1 1.9 fusion.38
  334.0 1.9 fusion.41
  335.9 3.4 collective-permute-start.13
  339.3 1.3 collective-permute-start.14
  340.6 0.0 collective-permute-done.13
  340.6 4.2 %collective-permute-done.14 = bf16[15,256]{1,0:T(8,128)(2,1)S(1)} collective-permute-done((bf16[15,256]{1,0:T(8,128)(2,1)S(1)}, bf16[15,256]{1,0:T(8,128)(2,1)S(1)}, u32[]{:S(2)}, u32[]{:S(2)}) %collective-permute-start.14) | collective-permute-done | bytes 7712 | tf_op jit(solution)/shard_map/ppermute | solution.py:17
  344.9 1.6 fusion.159
  346.5 5.9 %all-reduce = (f32[384,1]{0,1:T(1,128)S(1)}, f32[384,1]{0,1:T(1,128)S(1)}) all-reduce(f32[384,1]{0,1:T(1,128)S(1)} %broadcast_in_dim.25, f32[384,1]{0,1:T(1,128)S(1)} %broadcast_in_dim.26), channel_id=1, replica_groups=mesh['sp'=8,'tp'=4] {'tp'}, use_global_device_ids=true, to_apply=%region_14.16 | all-reduce | flops 768 | bytes 6144 | tf_op jit(solution)/shard_map/psum | solution.py:56
  352.5 3.0 convolution_convert_fusion
  355.5 28.2 %reduce-scatter.8.cloned.1.call-done = bf16[384,512]{1,0:T(8,128)(2,1)} async-done(((bf16[384,2048]{1,0:T(8,128)(2,1)}), bf16[384,512]{1,0:T(8,128)(2,1)}) %reduce-scatter.8.cloned.1.call-update) | async-done | bytes 393232 | tf_op jit(solution)/shard_map/reduce_scatter | solution.py:72
  383.7 1.8 add_convert_fusion
  (38 shorter events, 0.4 us)
Async XLA Ops:
  6.5 65.8 %all-gather.6.cloned.1.call-start = ((), (), s32[]{:S(2)}) async-start(), calls=%async_computation.4 | async-start | bytes 3538944 | tf_op jit(solution)/shard_map/all_gather | solution.py:31
  7.3 125.9 %all-gather.4.cloned.1.call-start = ((), (), s32[]{:S(2)}) async-start(), calls=%async_computation.3 | async-start | bytes 3538944 | tf_op jit(solution)/shard_map/all_gather | solution.py:30
  8.0 188.6 %all-gather.8.cloned.1.call-start = ((), (), s32[]{:S(2)}) async-start(), calls=%async_computation.5 | async-start | bytes 3538944 | tf_op jit(solution)/shard_map/all_gather | solution.py:33
  8.7 217.4 %reduce-scatter.4.cloned.1.call-start = ((), (), s32[]{:S(2)}) async-start(), calls=%async_computation.6 | async-start | bytes 1966080 | tf_op jit(solution)/shard_map/reduce_scatter | solution.py:72
  8.8 8.1 %collective-permute-start = (bf16[384,512]{1,0:T(8,128)(2,1)}, bf16[384,512]{1,0:T(8,128)(2,1)S(1)}, u32[]{:S(2)}, u32[]{:S(2)}) collective-permute-start(bf16[384,512]{1,0:T(8,128)(2,1)} %param.11), channel_id=1, source_target_pairs={{0,1},{1,2},{2,3},{3,0},{4,5},{5,6},{6,7},{7,4},{8,9},{9,10},{10,1... | collective-permute-start | bytes 1179656 | tf_op jit(solution)/shard_map/ppermute | solution.py:37
  16.9 7.2 %collective-permute-start.1 = (bf16[384,512]{1,0:T(8,128)(2,1)S(1)}, bf16[384,512]{1,0:T(8,128)(2,1)S(1)}, u32[]{:S(2)}, u32[]{:S(2)}) collective-permute-start(bf16[384,512]{1,0:T(8,128)(2,1)S(1)} %collective-permute-done), channel_id=1, source_target_pairs={{0,1},{1,2},{2,3},{3,0},{4,5},{5,6},{6,7},{7,4},{8,9},{9,10},{10,1... | collective-permute-start | bytes 1179656 | tf_op jit(solution)/shard_map/ppermute | solution.py:37
  24.1 7.2 %collective-permute-start.2 = (bf16[384,512]{1,0:T(8,128)(2,1)S(1)}, bf16[384,512]{1,0:T(8,128)(2,1)S(1)}, u32[]{:S(2)}, u32[]{:S(2)}) collective-permute-start(bf16[384,512]{1,0:T(8,128)(2,1)S(1)} %collective-permute-done.1), channel_id=1, source_target_pairs={{0,1},{1,2},{2,3},{3,0},{4,5},{5,6},{6,7},{7,4},{8,9},{9,10},{10,1... | collective-permute-start | bytes 1179656 | tf_op jit(solution)/shard_map/ppermute | solution.py:37
  74.2 64.7 %copy-start.2 = (f32[3,256]{1,0:T(4,128)S(1)}, f32[3,256]{1,0:T(4,128)}, u32[]{:S(2)}) copy-start(f32[3,256]{1,0:T(4,128)} %param.18) | copy-start | bytes 9220
  135.1 3.8 collective-permute-start.3
  137.6 5.9 %collective-permute-start.4 = (bf16[15,256]{1,0:T(8,128)(2,1)S(1)}, bf16[15,256]{1,0:T(8,128)(2,1)S(1)}, u32[]{:S(2)}, u32[]{:S(2)}) collective-permute-start(bf16[15,256]{1,0:T(8,128)(2,1)S(1)} %get-tuple-element.38), channel_id=1, source_target_pairs={{4,0},{8,4},{12,8},{16,12},{20,16},{24,20},{28,24},{5,1},{9,5},{13... | collective-permute-start | bytes 23048 | tf_op jit(solution)/shard_map/ppermute | solution.py:17
  145.2 80.9 %copy-start = (bf16[384,512]{1,0:T(8,128)(2,1)S(1)}, bf16[384,512]{1,0:T(8,128)(2,1)}, u32[]{:S(2)}) copy-start(bf16[384,512]{1,0:T(8,128)(2,1)} %param.11) | copy-start | bytes 1179652
  196.6 45.1 %copy-start.1 = (f32[3,31,256]{2,1,0:T(8,128)S(1)}, f32[3,31,256]{2,1,0:T(8,128)}, u32[]{:S(2)}) copy-start(f32[3,31,256]{2,1,0:T(8,128)} %param.15) | copy-start | bytes 285700
  199.7 105.2 %reduce-scatter.6.cloned.1.call-start = ((), (), s32[]{:S(2)}) async-start(), calls=%async_computation.7 | async-start | bytes 1966080 | tf_op jit(solution)/shard_map/reduce_scatter | solution.py:72
  227.2 7.3 %collective-permute-start.5 = (bf16[384,512]{1,0:T(8,128)(2,1)S(1)}, bf16[384,512]{1,0:T(8,128)(2,1)S(1)}, u32[]{:S(2)}, u32[]{:S(2)}) collective-permute-start(bf16[384,512]{1,0:T(8,128)(2,1)S(1)} %add_convert_fusion.2), channel_id=1, source_target_pairs={{0,1},{1,2},{2,3},{3,0},{4,5},{5,6},{6,7},{7,4},{8,9},{9,10},{10,1... | collective-permute-start | bytes 1179656 | tf_op jit(solution)/shard_map/ppermute | solution.py:37
  234.4 7.2 %collective-permute-start.6 = (bf16[384,512]{1,0:T(8,128)(2,1)S(1)}, bf16[384,512]{1,0:T(8,128)(2,1)S(1)}, u32[]{:S(2)}, u32[]{:S(2)}) collective-permute-start(bf16[384,512]{1,0:T(8,128)(2,1)S(1)} %collective-permute-done.5), channel_id=1, source_target_pairs={{0,1},{1,2},{2,3},{3,0},{4,5},{5,6},{6,7},{7,4},{8,9},{9,10},{10,1... | collective-permute-start | bytes 1179656 | tf_op jit(solution)/shard_map/ppermute | solution.py:37
  241.6 7.2 %collective-permute-start.7 = (bf16[384,512]{1,0:T(8,128)(2,1)S(1)}, bf16[384,512]{1,0:T(8,128)(2,1)S(1)}, u32[]{:S(2)}, u32[]{:S(2)}) collective-permute-start(bf16[384,512]{1,0:T(8,128)(2,1)S(1)} %collective-permute-done.6), channel_id=1, source_target_pairs={{0,1},{1,2},{2,3},{3,0},{4,5},{5,6},{6,7},{7,4},{8,9},{9,10},{10,1... | collective-permute-start | bytes 1179656 | tf_op jit(solution)/shard_map/ppermute | solution.py:37
  257.0 4.9 %collective-permute-start.8 = (bf16[15,256]{1,0:T(8,128)(2,1)S(1)}, bf16[15,256]{1,0:T(8,128)(2,1)S(1)}, u32[]{:S(2)}, u32[]{:S(2)}) collective-permute-start(bf16[15,256]{1,0:T(8,128)(2,1)S(1)} %get-tuple-element.35), channel_id=1, source_target_pairs={{0,4},{4,8},{8,12},{12,16},{16,20},{20,24},{24,28},{1,5},{5,9},{9,... | collective-permute-start | bytes 23048 | tf_op jit(solution)/shard_map/ppermute | solution.py:16
  260.4 5.5 %collective-permute-start.9 = (bf16[15,256]{1,0:T(8,128)(2,1)S(1)}, bf16[15,256]{1,0:T(8,128)(2,1)S(1)}, u32[]{:S(2)}, u32[]{:S(2)}) collective-permute-start(bf16[15,256]{1,0:T(8,128)(2,1)S(1)} %get-tuple-element.36), channel_id=1, source_target_pairs={{4,0},{8,4},{12,8},{16,12},{20,16},{24,20},{28,24},{5,1},{9,5},{13... | collective-permute-start | bytes 23048 | tf_op jit(solution)/shard_map/ppermute | solution.py:17
  276.8 107.0 %reduce-scatter.8.cloned.1.call-start = ((), (), s32[]{:S(2)}) async-start(), calls=%async_computation.8 | async-start | bytes 1966080 | tf_op jit(solution)/shard_map/reduce_scatter | solution.py:72
  306.0 7.3 %collective-permute-start.10 = (bf16[384,512]{1,0:T(8,128)(2,1)S(1)}, bf16[384,512]{1,0:T(8,128)(2,1)S(1)}, u32[]{:S(2)}, u32[]{:S(2)}) collective-permute-start(bf16[384,512]{1,0:T(8,128)(2,1)S(1)} %add_convert_fusion.1), channel_id=1, source_target_pairs={{0,1},{1,2},{2,3},{3,0},{4,5},{5,6},{6,7},{7,4},{8,9},{9,10},{10,1... | collective-permute-start | bytes 1179656 | tf_op jit(solution)/shard_map/ppermute | solution.py:37
  313.3 7.2 %collective-permute-start.11 = (bf16[384,512]{1,0:T(8,128)(2,1)S(1)}, bf16[384,512]{1,0:T(8,128)(2,1)S(1)}, u32[]{:S(2)}, u32[]{:S(2)}) collective-permute-start(bf16[384,512]{1,0:T(8,128)(2,1)S(1)} %collective-permute-done.10), channel_id=1, source_target_pairs={{0,1},{1,2},{2,3},{3,0},{4,5},{5,6},{6,7},{7,4},{8,9},{9,10},{10,1... | collective-permute-start | bytes 1179656 | tf_op jit(solution)/shard_map/ppermute | solution.py:37
  320.5 7.2 %collective-permute-start.12 = (bf16[384,512]{1,0:T(8,128)(2,1)S(1)}, bf16[384,512]{1,0:T(8,128)(2,1)S(1)}, u32[]{:S(2)}, u32[]{:S(2)}) collective-permute-start(bf16[384,512]{1,0:T(8,128)(2,1)S(1)} %collective-permute-done.11), channel_id=1, source_target_pairs={{0,1},{1,2},{2,3},{3,0},{4,5},{5,6},{6,7},{7,4},{8,9},{9,10},{10,1... | collective-permute-start | bytes 1179656 | tf_op jit(solution)/shard_map/ppermute | solution.py:37
  335.9 4.7 %collective-permute-start.13 = (bf16[15,256]{1,0:T(8,128)(2,1)S(1)}, bf16[15,256]{1,0:T(8,128)(2,1)S(1)}, u32[]{:S(2)}, u32[]{:S(2)}) collective-permute-start(bf16[15,256]{1,0:T(8,128)(2,1)S(1)} %get-tuple-element.33), channel_id=1, source_target_pairs={{0,4},{4,8},{8,12},{12,16},{16,20},{20,24},{24,28},{1,5},{5,9},{9,... | collective-permute-start | bytes 23048 | tf_op jit(solution)/shard_map/ppermute | solution.py:16
  339.3 5.5 %collective-permute-start.14 = (bf16[15,256]{1,0:T(8,128)(2,1)S(1)}, bf16[15,256]{1,0:T(8,128)(2,1)S(1)}, u32[]{:S(2)}, u32[]{:S(2)}) collective-permute-start(bf16[15,256]{1,0:T(8,128)(2,1)S(1)} %get-tuple-element.34), channel_id=1, source_target_pairs={{4,0},{8,4},{12,8},{16,12},{20,16},{24,20},{28,24},{5,1},{9,5},{13... | collective-permute-start | bytes 23048 | tf_op jit(solution)/shard_map/ppermute | solution.py:17
Sparse Core Ops, SparseCore 0:
  9.5 62.7 all-gather.5
  74.5 58.6 all-gather.3
  135.2 61.3 all-gather.7
  199.8 26.2 reduce-scatter.3
  276.9 28.0 reduce-scatter.5
  355.7 28.0 reduce-scatter.7
